TPU v7x, 32 devices: a whole 2x2x4 slice. The times are simulated.
32 devices in a mesh: ep: 8 (over z, x), tp: 4 (over y, core).
Axes of the slice: x: 2, y: 2, z: 4, core: 2. Of those that a mesh axis runs over, the one named last changes fastest.
Arguments:
- hidden_in: bfloat16 [256, 2048], P('ep', 'tp'), may hold values from -6 to 6
- state_in: float32 [256, 8, 128, 128], P('ep', 'tp'), may hold values from -0.6 to 0.6
- attn_gain: float32 [2048], replicated, may hold values from 0.1 to 1.9
- w_query: bfloat16 [2048, 1024], P(None, 'tp'), may hold values from -0.125 to 0.125
- w_key: bfloat16 [2048, 1024], P(None, 'tp'), may hold values from -0.125 to 0.125
- w_value: bfloat16 [2048, 1024], P(None, 'tp'), may hold values from -0.125 to 0.125
- w_gate: bfloat16 [2048, 1024], P(None, 'tp'), may hold values from -0.125 to 0.125
- w_beta: bfloat16 [2048, 8], replicated, may hold values from -0.125 to 0.125
- w_decay: bfloat16 [2048, 8], replicated, may hold values from -0.125 to 0.125
- decay_scale: float32 [8], replicated, may hold values from 0.05 to 3
- head_gain: float32 [128], replicated, may hold values from 0.1 to 1.9
- w_output: bfloat16 [1024, 2048], P(None, 'tp'), may hold values from -0.1875 to 0.1875
- ffn_gain: float32 [2048], replicated, may hold values from 0.1 to 1.9
- expert_ids: int32 [256, 2], P('ep'), may hold values from 0 to 7, all different within a row; in each aligned block of 32 rows (0 to 31, 32 to 63, ...) at most 16 rows name the same one
- route_weight: float32 [256, 2], P('ep'), may hold values from 0.2 to 1
- expert_gate: bfloat16 [8, 2048, 3072], P('ep', None, 'tp'), may hold values from -0.125 to 0.125
- expert_up: bfloat16 [8, 2048, 3072], P('ep', None, 'tp'), may hold values from -0.125 to 0.125
- expert_down: bfloat16 [8, 3072, 2048], P('ep', 'tp'), may hold values from -0.109375 to 0.109375
- dense_gate: bfloat16 [2048, 4096], P(None, 'ep'), may hold values from -0.125 to 0.125
- dense_up: bfloat16 [2048, 4096], P(None, 'ep'), may hold values from -0.125 to 0.125
- dense_down: bfloat16 [4096, 2048], P('ep'), may hold values from -0.09375 to 0.09375
- dense_mix: float32 [2048], P('tp'), may hold values from -6 to 6
Outputs:
- result: bfloat16 [256, 2048], P('ep', 'tp')
- new_state: float32 [256, 8, 128, 128], P('ep', 'tp')
Inputs may be any that keep to these rules, and one draw needn't show every extreme that they name: `expert_ids`: each row names 2 different experts. Within the rows of one index of ep (aligned blocks of 32 sequences) no expert is named more than 16 times, a bound that some block reaches.
All inputs are finite; a program needn't handle non-finite values.
Results may differ from a plain program's by a relative error of at most 0.015.
Values may be sent and summed in bfloat16 or wider, within the bound.
No kernel may reach another device: no remote copies, remote signals or barrier semaphores. Data moves between devices by JAX's collectives and lax.ppermute only.
A program may use at most 64 MiB of HBM per device.

v0:
```python
import jax
import jax.numpy as jnp
from jax import lax
from jax.sharding import PartitionSpec as P

EPS = 1e-06


def root_norm(values, scale_vec):
    wide = values.astype(jnp.float32)
    return wide * lax.rsqrt(jnp.mean(wide * wide, axis=-1, keepdims=True) + EPS) * scale_vec


def unit_norm(values):
    return values * lax.rsqrt(jnp.sum(values * values, axis=-1, keepdims=True) + EPS)


def slot_table(expert_ids, count):
    flat = expert_ids.reshape(-1)
    onehot = (flat[:, None] == jnp.arange(count, dtype=jnp.int32)[None, :]).astype(jnp.int32)
    before = jnp.cumsum(onehot, axis=0) - onehot
    return jnp.sum(before * onehot, axis=1).reshape(expert_ids.shape)


def delta_update(old_state, key_rows, value_rows, beta_rate, decay_rate):
    recalled = jnp.einsum("shk,shkv->shv", key_rows, old_state, precision=lax.Precision.HIGHEST)
    erased = (
        old_state - beta_rate[..., None, None] * key_rows[..., :, None] * recalled[..., None, :]
    )
    written = beta_rate[..., None, None] * key_rows[..., :, None] * value_rows[..., None, :]
    return decay_rate[..., None, None] * erased + written


def head_output(new_state, queries, gate_rows, head_gain):
    read = jnp.einsum("shk,shkv->shv", queries, new_state, precision=lax.Precision.HIGHEST)
    return (root_norm(read, head_gain) * jax.nn.silu(gate_rows)).astype(jnp.bfloat16)


def per_device(
    hidden_in,
    state_in,
    attn_gain,
    w_query,
    w_key,
    w_value,
    w_gate,
    w_beta,
    w_decay,
    decay_scale,
    head_gain,
    w_output,
    ffn_gain,
    expert_ids,
    route_weight,
    expert_gate,
    expert_up,
    expert_down,
    dense_gate,
    dense_up,
    dense_down,
    dense_mix,
):
    seq_dev = hidden_in.shape[0]
    tp_size = lax.axis_size("tp")
    ep_size = lax.axis_size("ep")
    tp_index = lax.axis_index("tp")
    local_heads = state_in.shape[1]
    key_dim = state_in.shape[2]
    value_dim = state_in.shape[3]
    local_width = hidden_in.shape[1]
    model_width = local_width * tp_size
    full_rows = lax.all_gather(hidden_in, "tp", axis=1, tiled=True)
    normed = root_norm(full_rows, attn_gain).astype(jnp.bfloat16)
    queries = unit_norm(
        jnp.dot(normed, w_query, preferred_element_type=jnp.float32).reshape(
            seq_dev, local_heads, key_dim
        )
    ) * key_dim ** (-0.5)
    key_rows = unit_norm(
        jnp.dot(normed, w_key, preferred_element_type=jnp.float32).reshape(
            seq_dev, local_heads, key_dim
        )
    )
    value_rows = jnp.dot(normed, w_value, preferred_element_type=jnp.float32).reshape(
        seq_dev, local_heads, value_dim
    )
    gate_rows = jnp.dot(normed, w_gate, preferred_element_type=jnp.float32).reshape(
        seq_dev, local_heads, value_dim
    )
    head_start = tp_index * local_heads
    beta_all = jnp.dot(normed, w_beta, preferred_element_type=jnp.float32)
    decay_all = jnp.dot(normed, w_decay, preferred_element_type=jnp.float32)
    beta_rate = jax.nn.sigmoid(lax.dynamic_slice_in_dim(beta_all, head_start, local_heads, 1))
    decay_logit = lax.dynamic_slice_in_dim(decay_all, head_start, local_heads, 1)
    decay_local = lax.dynamic_slice_in_dim(decay_scale, head_start, local_heads, 0)
    decay_rate = jnp.exp(-decay_local[None, :] * jax.nn.softplus(decay_logit))
    new_state = delta_update(state_in, key_rows, value_rows, beta_rate, decay_rate)
    heads_out = head_output(new_state, queries, gate_rows, head_gain).reshape(
        seq_dev, local_heads * value_dim
    )
    all_heads = lax.all_gather(heads_out, "tp", axis=1, tiled=True)
    mixed = (
        hidden_in.astype(jnp.float32)
        + jnp.dot(all_heads, w_output, preferred_element_type=jnp.float32)
    ).astype(jnp.bfloat16)
    block_rows = seq_dev // tp_size
    top_count = expert_ids.shape[1]
    experts_all = expert_gate.shape[0] * ep_size
    capacity = max(2, 2 * seq_dev * top_count // experts_all)
    slots = slot_table(expert_ids, experts_all)
    place = expert_ids * capacity + slots
    columns = jnp.arange(experts_all * capacity, dtype=jnp.int32)
    send_matrix = jnp.sum(
        (place[None, :, :] == columns[:, None, None]).astype(jnp.bfloat16), axis=2
    )
    take_matrix = jnp.sum(
        jnp.where(place[:, :, None] == columns[None, None, :], route_weight[:, :, None], 0.0),
        axis=1,
    )
    mixed_full = lax.all_gather(mixed, "tp", axis=1, tiled=True)
    normed2 = root_norm(mixed_full, ffn_gain).astype(jnp.bfloat16)
    dense_rows = lax.dynamic_slice_in_dim(normed2, tp_index * block_rows, block_rows, 0)
    outgoing = jnp.dot(send_matrix, normed2, preferred_element_type=jnp.float32).astype(
        jnp.bfloat16
    )
    outgoing = outgoing.reshape(experts_all, capacity, model_width)
    rows = lax.all_to_all(outgoing, "ep", split_axis=0, concat_axis=0, tiled=True)
    flat = rows.reshape(-1, rows.shape[2])
    gate_val = jnp.dot(flat, expert_gate[0], preferred_element_type=jnp.float32)
    up_val = jnp.dot(flat, expert_up[0], preferred_element_type=jnp.float32)
    inner = (jax.nn.silu(gate_val) * up_val).astype(jnp.bfloat16)
    partial_out = jnp.dot(inner, expert_down[0], preferred_element_type=jnp.float32).reshape(
        rows.shape
    )
    summed = lax.psum_scatter(
        partial_out.astype(jnp.bfloat16), "tp", scatter_dimension=2, tiled=True
    )
    returned = lax.all_to_all(summed, "ep", split_axis=0, concat_axis=0, tiled=True)
    moe_sum = jnp.dot(
        take_matrix,
        returned.reshape(-1, local_width).astype(jnp.float32),
        precision=lax.Precision.HIGHEST,
    )
    piece = lax.all_gather(dense_rows, "ep", axis=0, tiled=True)
    gate_val = jnp.dot(piece, dense_gate, preferred_element_type=jnp.float32)
    up_val = jnp.dot(piece, dense_up, preferred_element_type=jnp.float32)
    dense_hidden = (jax.nn.silu(gate_val) * up_val).astype(jnp.bfloat16)
    dense_own = lax.psum_scatter(
        jnp.dot(dense_hidden, dense_down, preferred_element_type=jnp.float32).astype(jnp.bfloat16),
        "ep",
        scatter_dimension=0,
        tiled=True,
    ).astype(jnp.float32)
    dense_out = lax.all_to_all(
        dense_own.astype(jnp.bfloat16), "tp", split_axis=1, concat_axis=0, tiled=True
    ).astype(dense_own.dtype)
    result = (
        mixed.astype(jnp.float32) + moe_sum + jax.nn.sigmoid(dense_mix)[None, :] * dense_out
    ).astype(jnp.bfloat16)
    return (result, new_state)


def solution(mesh):
    placed = (
        P("ep", "tp"),
        P("ep", "tp", None, None),
        P(),
        P(None, "tp"),
        P(None, "tp"),
        P(None, "tp"),
        P(None, "tp"),
        P(),
        P(),
        P(),
        P(),
        P(None, "tp"),
        P(),
        P("ep", None),
        P("ep", None),
        P("ep", None, "tp"),
        P("ep", None, "tp"),
        P("ep", "tp", None),
        P(None, "ep"),
        P(None, "ep"),
        P("ep", None),
        P("tp"),
    )
    return jax.shard_map(
        per_device,
        mesh=mesh,
        in_specs=placed,
        out_specs=(P("ep", "tp"), P("ep", "tp", None, None)),
        check_vma=False,
    )
```

profile of v0, /device:TPU:0, one launch (start us, length us, event | category | flops | bytes accessed | tf_op | source)
XLA Modules:
  0.0 204.3 jit_solution(7041996628087368338)
XLA Ops:
  7.2 0.0 copy-start
  7.2 0.0 copy-start.6
  7.2 6.9 %all_gather.12 = bf16[32,2048]{1,0:T(8,128)(2,1)S(1)} all-gather(bf16[32,512]{1,0:T(8,128)(2,1)} %param.22), channel_id=1, replica_groups=mesh['ep'=8,'tp'=4] {'tp'}, dimensions={1}, use_global_device_ids=true | all-gather | bytes 163840 | tf_op jit(solution)/shard_map/all_gather | solution.py:72
  14.1 0.1 fusion.19
  14.2 1.0 fusion.45
  15.2 1.0 fusion.47
  16.2 0.7 dynamic-slice_negate_fusion
  17.0 0.1 fusion.37
  17.0 0.1 copy.44
  17.1 1.6 fusion.43
  18.7 0.1 multiply_reduce_fusion.1
  18.8 0.1 copy.43
  18.9 1.6 fusion.41
  20.5 1.5 fusion.49
  22.1 0.0 copy-start.1
  22.1 0.1 multiply_reduce_fusion.2
  22.3 0.1 multiply_multiply_fusion
  22.4 0.1 broadcast_multiply_fusion.1
  22.5 5.5 %fusion.51 = f32[32,2,1,128]{3,2,1,0:T(1,128)S(1)} fusion(f32[32,2,128,1]{2,3,1,0:T(1,128)S(1)} %bitcast.72, f32[32,2,128,128]{3,2,1,0:T(8,128)} %param.23), kind=kOutput, calls=%fused_computation.74 | convolution fusion | flops 12582912 | bytes 4259840 | tf_op jit(solution)/shard_map/shk,shkv->shv/dot_general | solution.py:26
  28.0 1.5 multiply_add_fusion
  29.5 0.0 copy-start.2
  29.5 0.0 copy-start.3
  29.6 0.0 copy-start.7
  29.6 2.0 copy-done.2
  31.5 3.6 %fusion.52 = f32[32,2,1,128]{3,2,1,0:T(1,128)S(1)} fusion(f32[32,2,128,1]{2,3,1,0:T(1,128)S(1)} %bitcast.71, f32[32,2,128,128]{3,2,1,0:T(8,128)S(1)} %multiply_add_fusion), kind=kOutput, calls=%fused_computation.75 | convolution fusion | flops 12582912 | bytes 4259840 | tf_op jit(solution)/shard_map/shk,shkv->shv/dot_general | solution.py:35
  35.2 0.1 multiply_reduce_fusion
  35.3 0.3 fusion.39
  35.7 0.1 fusion.34
  35.8 5.4 %all_gather.13 = bf16[32,1024]{1,0:T(8,128)(2,1)S(1)} all-gather(bf16[32,256]{1,0:T(8,128)(2,1)S(1)} %bitcast.73), channel_id=1, replica_groups=mesh['ep'=8,'tp'=4] {'tp'}, dimensions={1}, use_global_device_ids=true | all-gather | bytes 81920 | tf_op jit(solution)/shard_map/all_gather | solution.py:101
  41.3 1.5 fusion.17
  42.8 0.6 copy-done.4
  43.4 5.4 %all_gather.14 = bf16[32,2048]{1,0:T(8,128)(2,1)S(1)} all-gather(bf16[32,512]{1,0:T(8,128)(2,1)S(1)} %fusion.17), channel_id=1, replica_groups=mesh['ep'=8,'tp'=4] {'tp'}, dimensions={1}, use_global_device_ids=true | all-gather | bytes 163840 | tf_op jit(solution)/shard_map/all_gather | solution.py:120
  48.8 0.1 fusion.22
  48.9 0.1 copy.45
  49.0 0.1 eq.20
  49.1 0.1 fusion.32
  49.2 0.1 reduce_window_sum.11
  49.3 0.2 select_reduce_fusion.1
  49.5 0.1 reshape.98
  49.6 0.1 copy.46
  49.7 0.1 fusion.35
  49.8 0.0 copy-done.8
  49.8 0.1 fusion.24
  49.9 1.1 convolution_convert_fusion
  51.0 6.0 %all-to-all-start = ((bf16[8,16,2048]{2,1,0:T(8,128)(2,1)}), bf16[8,16,2048]{2,1,0:T(8,128)(2,1)}, u32[]{:S(2)}, u32[]{:S(2)}) async-start(bf16[8,16,2048]{2,1,0:T(8,128)(2,1)} %bitcast.65), calls=%async_computation | async-start | bytes 1048576 | tf_op jit(solution)/shard_map/all_to_all | solution.py:127
  57.0 0.0 reduce-scatter.5.cloned.1.call-start
  57.1 38.0 %all_gather.15 = bf16[64,2048]{1,0:T(8,128)(2,1)S(1)} all-gather(bf16[8,2048]{1,0:T(8,128)(2,1)S(1)} %constant_dynamic-slice_fusion), channel_id=1, replica_groups=mesh['ep'=8,'tp'=4] {'ep'}, dimensions={0}, use_global_device_ids=true | all-gather | bytes 294912 | tf_op jit(solution)/shard_map/all_gather | solution.py:144
  95.0 2.1 %fusion.53 = f32[64,512]{1,0:T(8,128)S(1)} fusion(bf16[64,2048]{1,0:T(8,128)(2,1)S(1)} %all_gather.15, bf16[2048,512]{1,0:T(8,128)(2,1)} %param.40), kind=kOutput, calls=%fused_computation.76 | convolution fusion | flops 134217728 | bytes 2490368 | tf_op jit(solution)/shard_map/dot_general | solution.py:145
  97.1 3.9 %convolution_convert_fusion.1 = bf16[64,2048]{1,0:T(8,128)(2,1)} fusion(bf16[512,2048]{1,0:T(8,128)(2,1)} %param.42, bf16[64,2048]{1,0:T(8,128)(2,1)S(1)} %all_gather.15, bf16[2048,512]{1,0:T(8,128)(2,1)} %param.41, f32[64,512]{1,0:T(8,128)S(1)} %fusion.53), kind=kOutput, calls=%fused_computation.9 | convolution fusion | flops 268763136 | bytes 4849664 | tf_op jit(solution)/shard_map/dot_general | solution.py:149
  101.0 0.0 reduce-scatter.5.cloned.1.call-update
  101.0 0.0 reduce-scatter.3.cloned.1.call-start
  101.1 2.8 %fusion.4 = f32[128,768]{1,0:T(8,128)S(1)} fusion(bf16[128,2048]{1,0:T(8,128)(2,1)} %bitcast.9, bf16[1,2048,768]{2,1,0:T(8,128)(2,1)} %param.37), kind=kOutput, calls=%fused_computation.5 | convolution fusion | flops 402653184 | bytes 4063232 | tf_op jit(solution)/shard_map/dot_general | solution.py:129
  103.8 0.2 copy-done.13
  104.0 1.6 fusion.12
  105.7 0.0 copy-start.5
  105.7 1.4 fusion.6
  107.1 0.0 reduce-scatter.3.cloned.1.call-update
  107.1 53.4 %reduce-scatter.5.cloned.1.call-done = bf16[8,2048]{1,0:T(8,128)(2,1)} async-done(((bf16[64,2048]{1,0:T(8,128)(2,1)}), bf16[8,2048]{1,0:T(8,128)(2,1)}) %reduce-scatter.5.cloned.1.call-update) | async-done | bytes 32784 | tf_op jit(solution)/shard_map/reduce_scatter | solution.py:148
  160.6 7.2 %all_to_all.23 = bf16[8,4,512]{2,0,1:T(8,128)(2,1)S(1)} all-to-all(bf16[8,4,512]{2,0,1:T(8,128)(2,1)} %bitcast.75), channel_id=1, replica_groups=mesh['ep'=8,'tp'=4] {'tp'}, dimensions={1} | all-to-all | bytes 65536 | tf_op jit(solution)/shard_map/all_to_all | solution.py:154
  167.7 16.1 %reduce-scatter.3.cloned.1.call-done = bf16[8,16,512]{2,1,0:T(8,128)(2,1)} async-done(((bf16[8,16,2048]{2,1,0:T(8,128)(2,1)}), bf16[8,16,512]{2,1,0:T(8,128)(2,1)}) %reduce-scatter.3.cloned.1.call-update) | async-done | bytes 131088 | tf_op jit(solution)/shard_map/reduce_scatter | solution.py:135
  183.8 5.5 %all-to-all-start.1 = ((bf16[8,16,512]{2,1,0:T(8,128)(2,1)}), bf16[8,16,512]{2,1,0:T(8,128)(2,1)S(1)}, u32[]{:S(2)}, u32[]{:S(2)}) async-start(bf16[8,16,512]{2,1,0:T(8,128)(2,1)} %reduce-scatter.3.cloned.1.call-done), calls=%async_computation.2 | async-start | bytes 262144 | tf_op jit(solution)/shard_map/all_to_all | solution.py:138
  189.4 0.1 select_reduce_fusion
  189.5 7.2 %all-to-all-done.1 = bf16[8,16,512]{2,1,0:T(8,128)(2,1)S(1)} async-done(((bf16[8,16,512]{2,1,0:T(8,128)(2,1)}), bf16[8,16,512]{2,1,0:T(8,128)(2,1)S(1)}, u32[]{:S(2)}, u32[]{:S(2)}) %all-to-all-start.1) | async-done | bytes 131104 | tf_op jit(solution)/shard_map/all_to_all | solution.py:138
  196.7 0.8 fusion.18
  (31 shorter events, 0.2 us)
Async XLA Ops:
  7.2 98.6 %copy-start = (bf16[1,768,2048]{2,1,0:T(8,128)(2,1)S(1)}, bf16[1,768,2048]{2,1,0:T(8,128)(2,1)}, u32[]{:S(2)}) copy-start(bf16[1,768,2048]{2,1,0:T(8,128)(2,1)} %param.39) | copy-start | bytes 9437188
  7.2 13.3 %copy-start.6 = (f32[2048]{0:T(1024)S(1)}, f32[2048]{0:T(1024)}, u32[]{:S(2)}) copy-start(f32[2048]{0:T(1024)} %param.24) | copy-start | bytes 24580
  22.1 5.9 %copy-start.1 = (f32[32,2,128,128]{3,2,1,0:T(8,128)S(1)}, f32[32,2,128,128]{3,2,1,0:T(8,128)}, u32[]{:S(2)}) copy-start(f32[32,2,128,128]{3,2,1,0:T(8,128)} %param.23) | copy-start | bytes 12582916
  29.5 2.0 copy-start.2
  29.5 5.8 %copy-start.3 = (bf16[2048,256]{1,0:T(8,128)(2,1)S(1)}, bf16[2048,256]{1,0:T(8,128)(2,1)}, u32[]{:S(2)}) copy-start(bf16[2048,256]{1,0:T(8,128)(2,1)} %param.28) | copy-start | bytes 3145732
  29.6 6.2 %copy-start.12 = (f32[128]{0:T(128)S(1)}, f32[128]{0:T(128)}, u32[]{:S(2)}) copy-start(f32[128]{0:T(128)} %param.32) | copy-start | bytes 1540
  29.6 11.7 %copy-start.7 = (bf16[32,512]{1,0:T(8,128)(2,1)S(1)}, bf16[32,512]{1,0:T(8,128)(2,1)}, u32[]{:S(2)}) copy-start(bf16[32,512]{1,0:T(8,128)(2,1)} %param.22) | copy-start | bytes 98308
  31.5 17.4 %copy-start.9 = (s32[32,2]{0,1:T(2,128)S(1)}, s32[32,2]{0,1:T(2,128)}, u32[]{:S(2)}) copy-start(s32[32,2]{0,1:T(2,128)} %param.35) | copy-start | bytes 772
  31.5 18.2 %copy-start.8 = (f32[2048]{0:T(1024)S(1)}, f32[2048]{0:T(1024)}, u32[]{:S(2)}) copy-start(f32[2048]{0:T(1024)} %param.34) | copy-start | bytes 24580
  42.8 0.6 copy-start.4
  51.0 50.0 %all-to-all-start = ((bf16[8,16,2048]{2,1,0:T(8,128)(2,1)}), bf16[8,16,2048]{2,1,0:T(8,128)(2,1)}, u32[]{:S(2)}, u32[]{:S(2)}) async-start(bf16[8,16,2048]{2,1,0:T(8,128)(2,1)} %bitcast.65), calls=%async_computation | async-start | bytes 1048576 | tf_op jit(solution)/shard_map/all_to_all | solution.py:127
  57.0 103.6 %reduce-scatter.5.cloned.1.call-start = ((), (), s32[]{:S(2)}) async-start(), calls=%async_computation.6 | async-start | bytes 294912 | tf_op jit(solution)/shard_map/reduce_scatter | solution.py:148
  101.0 82.8 %reduce-scatter.3.cloned.1.call-start = ((), (), s32[]{:S(2)}) async-start(), calls=%async_computation.5 | async-start | bytes 655360 | tf_op jit(solution)/shard_map/reduce_scatter | solution.py:135
  101.0 3.0 %copy-start.13 = (bf16[1,2048,768]{2,1,0:T(8,128)(2,1)S(1)}, bf16[1,2048,768]{2,1,0:T(8,128)(2,1)}, u32[]{:S(2)}) copy-start(bf16[1,2048,768]{2,1,0:T(8,128)(2,1)} %param.38) | copy-start | bytes 9437188
  105.7 83.7 %copy-start.11 = (f32[32,2]{0,1:T(2,128)S(1)}, f32[32,2]{0,1:T(2,128)}, u32[]{:S(2)}) copy-start(f32[32,2]{0,1:T(2,128)} %param.36) | copy-start | bytes 772
  105.7 83.7 %copy-start.10 = (f32[512]{0:T(512)S(1)}, f32[512]{0:T(512)}, u32[]{:S(2)}) copy-start(f32[512]{0:T(512)} %param.43) | copy-start | bytes 6148
  105.7 91.0 %copy-start.5 = (bf16[32,512]{1,0:T(8,128)(2,1)S(1)}, bf16[32,512]{1,0:T(8,128)(2,1)}, u32[]{:S(2)}) copy-start(bf16[32,512]{1,0:T(8,128)(2,1)} %copy-done.4) | copy-start | bytes 98308
  183.8 12.9 %all-to-all-start.1 = ((bf16[8,16,512]{2,1,0:T(8,128)(2,1)}), bf16[8,16,512]{2,1,0:T(8,128)(2,1)S(1)}, u32[]{:S(2)}, u32[]{:S(2)}) async-start(bf16[8,16,512]{2,1,0:T(8,128)(2,1)} %reduce-scatter.3.cloned.1.call-done), calls=%async_computation.2 | async-start | bytes 262144 | tf_op jit(solution)/shard_map/all_to_all | solution.py:138
Sparse Core Ops, SparseCore 0:
  101.1 59.4 reduce-scatter.4
  163.1 20.7 reduce-scatter.2
where the time goes:
time: 205 us; the launch traced here: 204 us
  waiting for transfers between devices  76.8 us (37%)
  blocking collectives  62.8 us (31%)
  matrix products  31.3 us (15%)
  between operations  14.4 us (7%)
  starting transfers between devices  11.6 us (6%)
  other arithmetic  3.93 us (2%)
  local copies, waits for them, and re-layouts  3.54 us (2%)
    reduce_scatter x1, waiting for transfers between devices, per_device(): lax.psum_scatter(jnp.dot(dense_hidden, dense_down, preferred_element_type...  53.4 us
    all_gather x1, blocking collectives, per_device(): piece = lax.all_gather(dense_rows, 'ep', axis=0, tiled=True)  38 us
    reduce_scatter x1, waiting for transfers between devices, per_device(): lax.psum_scatter(partial_out.astype(jnp.bfloat16), 'tp', scatter_dimensio...  16.1 us
    all_to_all x1, waiting for transfers between devices, per_device(): lax.all_to_all(summed, 'ep', split_axis=0, concat_axis=0, tiled=True)  7.23 us
    all_to_all x1, blocking collectives, per_device(): lax.all_to_all(dense_own.astype(jnp.bfloat16), 'tp', split_axis=1, concat...  7.17 us
    all_gather x1, blocking collectives, per_device(): full_rows = lax.all_gather(hidden_in, 'tp', axis=1, tiled=True)  6.88 us
    all_to_all x1, starting transfers between devices, per_device(): lax.all_to_all(outgoing, 'ep', split_axis=0, concat_axis=0, tiled=True)  5.98 us
    all_to_all x1, starting transfers between devices, per_device(): lax.all_to_all(summed, 'ep', split_axis=0, concat_axis=0, tiled=True)  5.53 us
  transfers between devices with their start and end apart: 4, of which 3 were waited for; matrix products, arithmetic and copies ran while one was open for 6% of the time, Pallas kernels for 0%

commit v1 on v0

--- a/solution.py
+++ b/solution.py
@@ -4,6 +4,17 @@
 from jax.sharding import PartitionSpec as P
 
 EPS = 1e-06
+
+
+def around_the_ring(x, mesh_axis, dim):
+    n_dev = lax.axis_size(mesh_axis)
+    hops = [(i, (i + 1) % n_dev) for i in range(n_dev)]
+    parts = [x]
+    for reach in range(1, n_dev):
+        parts = [lax.ppermute(parts[0], mesh_axis, hops), *parts]
+    out = jnp.concatenate(parts, axis=dim)
+    places = (lax.axis_index(mesh_axis) + 1) * parts[-1].shape[dim]
+    return jnp.roll(out, places, axis=dim)
 
 
 def root_norm(values, scale_vec):
@@ -141,7 +152,7 @@
         returned.reshape(-1, local_width).astype(jnp.float32),
         precision=lax.Precision.HIGHEST,
     )
-    piece = lax.all_gather(dense_rows, "ep", axis=0, tiled=True)
+    piece = around_the_ring(dense_rows, "ep", 0)
     gate_val = jnp.dot(piece, dense_gate, preferred_element_type=jnp.float32)
     up_val = jnp.dot(piece, dense_up, preferred_element_type=jnp.float32)
     dense_hidden = (jax.nn.silu(gate_val) * up_val).astype(jnp.bfloat16)

time: 205 us -> 211 us (1.029)
  waiting for transfers between devices: 76.8 us -> 118 us
  blocking collectives: 62.8 us -> 24.9 us
    all_gather x1 -> x0, blocking collectives: 38 us -> none  [per_device(): piece = lax.all_gather(dense_rows, 'ep', axis=0, tiled=True)]
    ppermute x0 -> x7, waiting for transfers between devices: none -> 37.2 us  [around_the_ring(): parts = [lax.ppermute(parts[0], mesh_axis, hops), *parts]]
    all_to_all x1, waiting for transfers between devices: 0.01 us -> 3.18 us  [per_device(): lax.all_to_all(outgoing, 'ep', split_axis=0, concat_axis=0, tiled=True)]
  transfers between devices with their start and end apart: 4 -> 11, of which waited for: 3 -> 10; matrix products, arithmetic and copies ran while one was open for 6% -> 7% of each run, Pallas kernels for 0% -> 0%
where the time goes in v1:
time: 211 us; the launch traced here: 210 us
  waiting for transfers between devices  118 us (56%)
  matrix products  31.4 us (15%)
  blocking collectives  24.9 us (12%)
  between operations  14.5 us (7%)
  starting transfers between devices  13.3 us (6%)
  other arithmetic  3.91 us (2%)
  local copies, waits for them, and re-layouts  3.8 us (2%)
    reduce_scatter x1, waiting for transfers between devices, per_device(): lax.psum_scatter(jnp.dot(dense_hidden, dense_down, preferred_element_type...  54.5 us
    ppermute x7, waiting for transfers between devices, around_the_ring(): parts = [lax.ppermute(parts[0], mesh_axis, hops), *parts]  37.2 us
    reduce_scatter x1, waiting for transfers between devices, per_device(): lax.psum_scatter(partial_out.astype(jnp.bfloat16), 'tp', scatter_dimensio...  16 us
    all_to_all x1, waiting for transfers between devices, per_device(): lax.all_to_all(summed, 'ep', split_axis=0, concat_axis=0, tiled=True)  7.23 us
    all_to_all x1, blocking collectives, per_device(): lax.all_to_all(dense_own.astype(jnp.bfloat16), 'tp', split_axis=1, concat...  7.17 us
    all_gather x1, blocking collectives, per_device(): full_rows = lax.all_gather(hidden_in, 'tp', axis=1, tiled=True)  6.88 us
    all_to_all x1, starting transfers between devices, per_device(): lax.all_to_all(outgoing, 'ep', split_axis=0, concat_axis=0, tiled=True)  6 us
    all_to_all x1, starting transfers between devices, per_device(): lax.all_to_all(summed, 'ep', split_axis=0, concat_axis=0, tiled=True)  5.51 us
  transfers between devices with their start and end apart: 11, of which 10 were waited for; matrix products, arithmetic and copies ran while one was open for 7% of the time, Pallas kernels for 0%

profile of v1, /device:TPU:0, one launch (start us, length us, event | category | flops | bytes accessed | tf_op | source)
XLA Modules:
  0.0 209.9 jit_solution(724918988436289061)
XLA Ops:
  7.2 0.0 copy-start
  7.2 6.9 %all_gather.9 = bf16[32,2048]{1,0:T(8,128)(2,1)S(1)} all-gather(bf16[32,512]{1,0:T(8,128)(2,1)} %param.22), channel_id=1, replica_groups=mesh['ep'=8,'tp'=4] {'tp'}, dimensions={1}, use_global_device_ids=true | all-gather | bytes 163840 | tf_op jit(solution)/shard_map/all_gather | solution.py:83
  14.1 0.1 fusion.18
  14.2 1.0 fusion.50
  15.2 1.0 fusion.52
  16.2 0.7 dynamic-slice_negate_fusion
  17.0 0.1 fusion.39
  17.0 0.1 copy.44
  17.1 1.6 fusion.48
  18.7 0.1 multiply_reduce_fusion.1
  18.8 0.1 copy.43
  18.9 1.6 fusion.46
  20.5 1.5 fusion.54
  22.1 0.1 multiply_reduce_fusion.2
  22.3 0.1 multiply_multiply_fusion
  22.4 0.1 broadcast_multiply_fusion.1
  22.5 5.5 %fusion.56 = f32[32,2,1,128]{3,2,1,0:T(1,128)S(1)} fusion(f32[32,2,128,1]{2,3,1,0:T(1,128)S(1)} %bitcast.70, f32[32,2,128,128]{3,2,1,0:T(8,128)} %param.23), kind=kOutput, calls=%fused_computation.90 | convolution fusion | flops 12582912 | bytes 4259840 | tf_op jit(solution)/shard_map/shk,shkv->shv/dot_general | solution.py:37
  28.0 1.5 multiply_add_fusion
  29.6 2.0 copy-done.2
  31.5 3.6 %fusion.57 = f32[32,2,1,128]{3,2,1,0:T(1,128)S(1)} fusion(f32[32,2,128,1]{2,3,1,0:T(1,128)S(1)} %bitcast.69, f32[32,2,128,128]{3,2,1,0:T(8,128)S(1)} %multiply_add_fusion), kind=kOutput, calls=%fused_computation.91 | convolution fusion | flops 12582912 | bytes 4259840 | tf_op jit(solution)/shard_map/shk,shkv->shv/dot_general | solution.py:46
  35.2 0.1 multiply_reduce_fusion
  35.3 0.3 fusion.44
  35.7 0.1 fusion.36
  35.8 5.4 %all_gather.10 = bf16[32,1024]{1,0:T(8,128)(2,1)S(1)} all-gather(bf16[32,256]{1,0:T(8,128)(2,1)S(1)} %bitcast.71), channel_id=1, replica_groups=mesh['ep'=8,'tp'=4] {'tp'}, dimensions={1}, use_global_device_ids=true | all-gather | bytes 81920 | tf_op jit(solution)/shard_map/all_gather | solution.py:112
  41.3 1.5 fusion.16
  42.8 5.4 %all_gather.11 = bf16[32,2048]{1,0:T(8,128)(2,1)S(1)} all-gather(bf16[32,512]{1,0:T(8,128)(2,1)S(1)} %fusion.16), channel_id=1, replica_groups=mesh['ep'=8,'tp'=4] {'tp'}, dimensions={1}, use_global_device_ids=true | all-gather | bytes 163840 | tf_op jit(solution)/shard_map/all_gather | solution.py:131
  48.2 0.1 fusion.21
  48.3 0.1 fusion.23
  48.4 1.7 collective-permute-start
  50.2 4.9 %collective-permute-done = bf16[8,2048]{1,0:T(8,128)(2,1)S(1)} collective-permute-done((bf16[8,2048]{1,0:T(8,128)(2,1)S(1)}, bf16[8,2048]{1,0:T(8,128)(2,1)S(1)}, u32[]{:S(2)}, u32[]{:S(2)}) %collective-permute-start) | collective-permute-done | bytes 32800 | tf_op jit(solution)/shard_map/ppermute | solution.py:14
  55.1 0.1 copy.45
  55.2 0.1 eq.44
  55.3 6.4 %collective-permute-done.1 = bf16[8,2048]{1,0:T(8,128)(2,1)S(1)} collective-permute-done((bf16[8,2048]{1,0:T(8,128)(2,1)S(1)}, bf16[8,2048]{1,0:T(8,128)(2,1)S(1)}, u32[]{:S(2)}, u32[]{:S(2)}) %collective-permute-start.1) | collective-permute-done | bytes 32800 | tf_op jit(solution)/shard_map/ppermute | solution.py:14
  61.7 0.1 fusion.34
  61.8 0.1 reduce_window_sum.11
  61.9 6.4 %collective-permute-done.2 = bf16[8,2048]{1,0:T(8,128)(2,1)S(1)} collective-permute-done((bf16[8,2048]{1,0:T(8,128)(2,1)S(1)}, bf16[8,2048]{1,0:T(8,128)(2,1)S(1)}, u32[]{:S(2)}, u32[]{:S(2)}) %collective-permute-start.2) | collective-permute-done | bytes 32800 | tf_op jit(solution)/shard_map/ppermute | solution.py:14
  68.3 0.2 select_reduce_fusion.1
  68.5 0.1 reshape.98
  68.6 0.1 copy.46
  68.7 6.2 %collective-permute-done.3 = bf16[8,2048]{1,0:T(8,128)(2,1)S(1)} collective-permute-done((bf16[8,2048]{1,0:T(8,128)(2,1)S(1)}, bf16[8,2048]{1,0:T(8,128)(2,1)S(1)}, u32[]{:S(2)}, u32[]{:S(2)}) %collective-permute-start.3) | collective-permute-done | bytes 32800 | tf_op jit(solution)/shard_map/ppermute | solution.py:14
  75.0 6.6 %collective-permute-done.4 = bf16[8,2048]{1,0:T(8,128)(2,1)S(1)} collective-permute-done((bf16[8,2048]{1,0:T(8,128)(2,1)S(1)}, bf16[8,2048]{1,0:T(8,128)(2,1)S(1)}, u32[]{:S(2)}, u32[]{:S(2)}) %collective-permute-start.4) | collective-permute-done | bytes 32800 | tf_op jit(solution)/shard_map/ppermute | solution.py:14
  81.6 0.1 fusion.37
  81.6 6.5 %collective-permute-done.5 = bf16[8,2048]{1,0:T(8,128)(2,1)S(1)} collective-permute-done((bf16[8,2048]{1,0:T(8,128)(2,1)S(1)}, bf16[8,2048]{1,0:T(8,128)(2,1)S(1)}, u32[]{:S(2)}, u32[]{:S(2)}) %collective-permute-start.5) | collective-permute-done | bytes 32800 | tf_op jit(solution)/shard_map/ppermute | solution.py:14
  88.2 1.1 convolution_convert_fusion
  89.3 6.0 %all-to-all-start = ((bf16[8,16,2048]{2,1,0:T(8,128)(2,1)}), bf16[8,16,2048]{2,1,0:T(8,128)(2,1)}, u32[]{:S(2)}, u32[]{:S(2)}) async-start(bf16[8,16,2048]{2,1,0:T(8,128)(2,1)} %bitcast.63), calls=%async_computation | async-start | bytes 1048576 | tf_op jit(solution)/shard_map/all_to_all | solution.py:138
  95.3 0.0 reduce-scatter.5.cloned.1.call-start
  95.6 0.8 copy-done.4
  96.4 2.1 fusion.24
  98.5 4.0 %convolution_convert_fusion.1 = bf16[64,2048]{1,0:T(8,128)(2,1)} fusion(bf16[512,2048]{1,0:T(8,128)(2,1)} %param.42, f32[64,512]{1,0:T(8,128)S(1)} %fusion.24, bf16[2048,512]{1,0:T(8,128)(2,1)} %param.40, bf16[128,2048]{1,0:T(8,128)(2,1)} %copy-done.4, s32[]{:T(128)S(6)} %select_n.34), kind=kOutput, calls=%fused_computation.9 | convolution fusion | flops 268763136 | bytes 4849668 | tf_op jit(solution)/shard_map/dot_general | solution.py:160
  102.4 0.0 reduce-scatter.5.cloned.1.call-update
  102.5 0.0 reduce-scatter.3.cloned.1.call-start
  102.5 3.2 %all-to-all-done = bf16[8,16,2048]{2,1,0:T(8,128)(2,1)} async-done(((bf16[8,16,2048]{2,1,0:T(8,128)(2,1)}), bf16[8,16,2048]{2,1,0:T(8,128)(2,1)}, u32[]{:S(2)}, u32[]{:S(2)}) %all-to-all-start) | async-done | bytes 524320 | tf_op jit(solution)/shard_map/all_to_all | solution.py:138
  105.7 2.8 %fusion.4 = f32[128,768]{1,0:T(8,128)S(1)} fusion(bf16[128,2048]{1,0:T(8,128)(2,1)} %bitcast.9, bf16[1,2048,768]{2,1,0:T(8,128)(2,1)} %param.37), kind=kOutput, calls=%fused_computation.5 | convolution fusion | flops 402653184 | bytes 4063232 | tf_op jit(solution)/shard_map/dot_general | solution.py:140
  108.5 0.2 copy-done.12
  108.7 1.6 fusion.12
  110.4 1.4 fusion.6
  111.7 0.0 reduce-scatter.3.cloned.1.call-update
  111.8 54.5 %reduce-scatter.5.cloned.1.call-done = bf16[8,2048]{1,0:T(8,128)(2,1)} async-done(((bf16[64,2048]{1,0:T(8,128)(2,1)}), bf16[8,2048]{1,0:T(8,128)(2,1)}) %reduce-scatter.5.cloned.1.call-update) | async-done | bytes 32784 | tf_op jit(solution)/shard_map/reduce_scatter | solution.py:159
  166.3 7.2 %all_to_all.23 = bf16[8,4,512]{2,0,1:T(8,128)(2,1)S(1)} all-to-all(bf16[8,4,512]{2,0,1:T(8,128)(2,1)} %bitcast.73), channel_id=1, replica_groups=mesh['ep'=8,'tp'=4] {'tp'}, dimensions={1} | all-to-all | bytes 65536 | tf_op jit(solution)/shard_map/all_to_all | solution.py:165
  173.4 16.0 %reduce-scatter.3.cloned.1.call-done = bf16[8,16,512]{2,1,0:T(8,128)(2,1)} async-done(((bf16[8,16,2048]{2,1,0:T(8,128)(2,1)}), bf16[8,16,512]{2,1,0:T(8,128)(2,1)}) %reduce-scatter.3.cloned.1.call-update) | async-done | bytes 131088 | tf_op jit(solution)/shard_map/reduce_scatter | solution.py:146
  189.4 5.5 %all-to-all-start.1 = ((bf16[8,16,512]{2,1,0:T(8,128)(2,1)}), bf16[8,16,512]{2,1,0:T(8,128)(2,1)S(1)}, u32[]{:S(2)}, u32[]{:S(2)}) async-start(bf16[8,16,512]{2,1,0:T(8,128)(2,1)} %reduce-scatter.3.cloned.1.call-done), calls=%async_computation.2 | async-start | bytes 262144 | tf_op jit(solution)/shard_map/all_to_all | solution.py:149
  194.9 0.1 select_reduce_fusion
  195.1 7.2 %all-to-all-done.1 = bf16[8,16,512]{2,1,0:T(8,128)(2,1)S(1)} async-done(((bf16[8,16,512]{2,1,0:T(8,128)(2,1)}), bf16[8,16,512]{2,1,0:T(8,128)(2,1)S(1)}, u32[]{:S(2)}, u32[]{:S(2)}) %all-to-all-start.1) | async-done | bytes 131104 | tf_op jit(solution)/shard_map/all_to_all | solution.py:149
  202.3 0.8 fusion.17
  (58 shorter events, 0.3 us)
Async XLA Ops:
  7.2 103.2 %copy-start = (bf16[1,768,2048]{2,1,0:T(8,128)(2,1)S(1)}, bf16[1,768,2048]{2,1,0:T(8,128)(2,1)}, u32[]{:S(2)}) copy-start(bf16[1,768,2048]{2,1,0:T(8,128)(2,1)} %param.39) | copy-start | bytes 9437188
  7.2 13.3 %copy-start.5 = (f32[2048]{0:T(1024)S(1)}, f32[2048]{0:T(1024)}, u32[]{:S(2)}) copy-start(f32[2048]{0:T(1024)} %param.24) | copy-start | bytes 24580
  22.1 5.9 %copy-start.1 = (f32[32,2,128,128]{3,2,1,0:T(8,128)S(1)}, f32[32,2,128,128]{3,2,1,0:T(8,128)}, u32[]{:S(2)}) copy-start(f32[32,2,128,128]{3,2,1,0:T(8,128)} %param.23) | copy-start | bytes 12582916
  29.5 2.0 copy-start.2
  29.5 5.8 %copy-start.3 = (bf16[2048,256]{1,0:T(8,128)(2,1)S(1)}, bf16[2048,256]{1,0:T(8,128)(2,1)}, u32[]{:S(2)}) copy-start(bf16[2048,256]{1,0:T(8,128)(2,1)} %param.28) | copy-start | bytes 3145732
  29.6 6.2 %copy-start.11 = (f32[128]{0:T(128)S(1)}, f32[128]{0:T(128)}, u32[]{:S(2)}) copy-start(f32[128]{0:T(128)} %param.32) | copy-start | bytes 1540
  29.6 11.7 %copy-start.6 = (bf16[32,512]{1,0:T(8,128)(2,1)S(1)}, bf16[32,512]{1,0:T(8,128)(2,1)}, u32[]{:S(2)}) copy-start(bf16[32,512]{1,0:T(8,128)(2,1)} %param.22) | copy-start | bytes 98308
  31.5 16.8 %copy-start.7 = (f32[2048]{0:T(1024)S(1)}, f32[2048]{0:T(1024)}, u32[]{:S(2)}) copy-start(f32[2048]{0:T(1024)} %param.34) | copy-start | bytes 24580
  31.5 23.6 %copy-start.8 = (s32[32,2]{0,1:T(2,128)S(1)}, s32[32,2]{0,1:T(2,128)}, u32[]{:S(2)}) copy-start(s32[32,2]{0,1:T(2,128)} %param.35) | copy-start | bytes 772
  48.4 6.7 %collective-permute-start = (bf16[8,2048]{1,0:T(8,128)(2,1)S(1)}, bf16[8,2048]{1,0:T(8,128)(2,1)S(1)}, u32[]{:S(2)}, u32[]{:S(2)}) collective-permute-start(bf16[8,2048]{1,0:T(8,128)(2,1)S(1)} %constant_dynamic-slice_fusion), channel_id=1, source_target_pairs={{0,4},{4,8},{8,12},{12,16},{16,20},{20,24},{24,28},{28,0},{1,5},{5... | collective-permute-start | bytes 98312 | tf_op jit(solution)/shard_map/ppermute | solution.py:14
  55.1 6.6 %collective-permute-start.1 = (bf16[8,2048]{1,0:T(8,128)(2,1)S(1)}, bf16[8,2048]{1,0:T(8,128)(2,1)S(1)}, u32[]{:S(2)}, u32[]{:S(2)}) collective-permute-start(bf16[8,2048]{1,0:T(8,128)(2,1)S(1)} %collective-permute-done), channel_id=1, source_target_pairs={{0,4},{4,8},{8,12},{12,16},{16,20},{20,24},{24,28},{28,0},{1,5},{5... | collective-permute-start | bytes 98312 | tf_op jit(solution)/shard_map/ppermute | solution.py:14
  61.7 6.6 %collective-permute-start.2 = (bf16[8,2048]{1,0:T(8,128)(2,1)S(1)}, bf16[8,2048]{1,0:T(8,128)(2,1)S(1)}, u32[]{:S(2)}, u32[]{:S(2)}) collective-permute-start(bf16[8,2048]{1,0:T(8,128)(2,1)S(1)} %collective-permute-done.1), channel_id=1, source_target_pairs={{0,4},{4,8},{8,12},{12,16},{16,20},{20,24},{24,28},{28,0},{1,5},{5... | collective-permute-start | bytes 98312 | tf_op jit(solution)/shard_map/ppermute | solution.py:14
  68.3 6.6 %collective-permute-start.3 = (bf16[8,2048]{1,0:T(8,128)(2,1)S(1)}, bf16[8,2048]{1,0:T(8,128)(2,1)S(1)}, u32[]{:S(2)}, u32[]{:S(2)}) collective-permute-start(bf16[8,2048]{1,0:T(8,128)(2,1)S(1)} %collective-permute-done.2), channel_id=1, source_target_pairs={{0,4},{4,8},{8,12},{12,16},{16,20},{20,24},{24,28},{28,0},{1,5},{5... | collective-permute-start | bytes 98312 | tf_op jit(solution)/shard_map/ppermute | solution.py:14
  74.9 6.6 %collective-permute-start.4 = (bf16[8,2048]{1,0:T(8,128)(2,1)S(1)}, bf16[8,2048]{1,0:T(8,128)(2,1)S(1)}, u32[]{:S(2)}, u32[]{:S(2)}) collective-permute-start(bf16[8,2048]{1,0:T(8,128)(2,1)S(1)} %collective-permute-done.3), channel_id=1, source_target_pairs={{0,4},{4,8},{8,12},{12,16},{16,20},{20,24},{24,28},{28,0},{1,5},{5... | collective-permute-start | bytes 98312 | tf_op jit(solution)/shard_map/ppermute | solution.py:14
  81.6 6.6 %collective-permute-start.5 = (bf16[8,2048]{1,0:T(8,128)(2,1)S(1)}, bf16[8,2048]{1,0:T(8,128)(2,1)S(1)}, u32[]{:S(2)}, u32[]{:S(2)}) collective-permute-start(bf16[8,2048]{1,0:T(8,128)(2,1)S(1)} %collective-permute-done.4), channel_id=1, source_target_pairs={{0,4},{4,8},{8,12},{12,16},{16,20},{20,24},{24,28},{28,0},{1,5},{5... | collective-permute-start | bytes 98312 | tf_op jit(solution)/shard_map/ppermute | solution.py:14
  88.2 7.2 %collective-permute-start.6 = (bf16[8,2048]{1,0:T(8,128)(2,1)S(1)}, bf16[8,2048]{1,0:T(8,128)(2,1)S(1)}, u32[]{:S(2)}, u32[]{:S(2)}) collective-permute-start(bf16[8,2048]{1,0:T(8,128)(2,1)S(1)} %collective-permute-done.5), channel_id=1, source_target_pairs={{0,4},{4,8},{8,12},{12,16},{16,20},{20,24},{24,28},{28,0},{1,5},{5... | collective-permute-start | bytes 98312 | tf_op jit(solution)/shard_map/ppermute | solution.py:14
  89.3 16.4 %all-to-all-start = ((bf16[8,16,2048]{2,1,0:T(8,128)(2,1)}), bf16[8,16,2048]{2,1,0:T(8,128)(2,1)}, u32[]{:S(2)}, u32[]{:S(2)}) async-start(bf16[8,16,2048]{2,1,0:T(8,128)(2,1)} %bitcast.63), calls=%async_computation | async-start | bytes 1048576 | tf_op jit(solution)/shard_map/all_to_all | solution.py:138
  95.3 71.0 %reduce-scatter.5.cloned.1.call-start = ((), (), s32[]{:S(2)}) async-start(), calls=%async_computation.6 | async-start | bytes 294912 | tf_op jit(solution)/shard_map/reduce_scatter | solution.py:159
  95.6 0.8 copy-start.4
  102.5 87.0 %reduce-scatter.3.cloned.1.call-start = ((), (), s32[]{:S(2)}) async-start(), calls=%async_computation.5 | async-start | bytes 655360 | tf_op jit(solution)/shard_map/reduce_scatter | solution.py:146
  105.7 3.0 %copy-start.12 = (bf16[1,2048,768]{2,1,0:T(8,128)(2,1)S(1)}, bf16[1,2048,768]{2,1,0:T(8,128)(2,1)}, u32[]{:S(2)}) copy-start(bf16[1,2048,768]{2,1,0:T(8,128)(2,1)} %param.38) | copy-start | bytes 9437188
  110.3 84.6 %copy-start.10 = (f32[32,2]{0,1:T(2,128)S(1)}, f32[32,2]{0,1:T(2,128)}, u32[]{:S(2)}) copy-start(f32[32,2]{0,1:T(2,128)} %param.36) | copy-start | bytes 772
  110.3 84.7 %copy-start.9 = (f32[512]{0:T(512)S(1)}, f32[512]{0:T(512)}, u32[]{:S(2)}) copy-start(f32[512]{0:T(512)} %param.43) | copy-start | bytes 6148
  189.4 12.9 %all-to-all-start.1 = ((bf16[8,16,512]{2,1,0:T(8,128)(2,1)}), bf16[8,16,512]{2,1,0:T(8,128)(2,1)S(1)}, u32[]{:S(2)}, u32[]{:S(2)}) async-start(bf16[8,16,512]{2,1,0:T(8,128)(2,1)} %reduce-scatter.3.cloned.1.call-done), calls=%async_computation.2 | async-start | bytes 262144 | tf_op jit(solution)/shard_map/all_to_all | solution.py:149
Sparse Core Ops, SparseCore 0:
  102.6 63.6 reduce-scatter.4
  168.8 20.6 reduce-scatter.2
